TPU v7x, 32 devices: a whole 2x2x4 slice. The times are simulated.
32 devices in a mesh: rep: 2 (over x), fs: 8 (over z, y), tp: 2 (over core).
Axes of the slice: x: 2, y: 2, z: 4, core: 2. Of those that a mesh axis runs over, the one named last changes fastest.
Arguments:
- tokens: bfloat16 [8192, 2048], P(('rep', 'fs')), may hold values from -6 to 6
- mix_gain: bfloat16 [2048], replicated, may hold values from 0.099609375 to 1.8984375
- value_weight: bfloat16 [2048, 1536], P('fs', 'tp'), may hold values from -0.125 to 0.125
- outer_gate_weight: bfloat16 [2048, 1536], P('fs', 'tp'), may hold values from -0.125 to 0.125
- inner_gate_weight: bfloat16 [2048, 1536], P('fs', 'tp'), may hold values from -0.125 to 0.125
- conv_taps: bfloat16 [3, 1536], P(None, 'tp'), may hold values from -3 to 3
- mix_out_weight: bfloat16 [1536, 2048], P('tp', 'fs'), may hold values from -0.15625 to 0.15625
- ffn_gain: bfloat16 [2048], replicated, may hold values from 0.099609375 to 1.8984375
- gate_weight: bfloat16 [2048, 4096], P('fs', 'tp'), may hold values from -0.125 to 0.125
- up_weight: bfloat16 [2048, 4096], P('fs', 'tp'), may hold values from -0.125 to 0.125
- down_weight: bfloat16 [4096, 2048], P('tp', 'fs'), may hold values from -0.09375 to 0.09375
Outputs:
- layer_out: bfloat16 [8192, 2048], P(('rep', 'fs'))
All inputs are finite; a program needn't handle non-finite values.
Results may differ from a plain program's by a relative error of at most 0.02.
Values may be sent and summed in bfloat16 or wider, within the bound.
A program may use at most 128 MiB of HBM per device.

v0:
```python
import jax
import jax.numpy as jnp
from jax import lax
from jax.sharding import PartitionSpec as P

SEQ_GRP = 2
EPS = 1e-05


def rms_norm(values, gain):
    floats = values.astype(jnp.float32)
    scaled = floats * lax.rsqrt(jnp.mean(floats * floats, axis=-1, keepdims=True) + EPS)
    return (scaled * gain.astype(jnp.float32)).astype(jnp.bfloat16)


def short_conv(value_proj, outer_proj, inner_proj, conv_taps, seq_len):
    mixed_in = inner_proj.astype(jnp.float32) * value_proj.astype(jnp.float32)
    count_rows = mixed_in.shape[0]
    position = (jnp.arange(count_rows, dtype=jnp.int32) % seq_len)[:, None]
    zero_row = jnp.zeros((1, mixed_in.shape[1]), jnp.float32)
    back_one = jnp.where(position >= 1, jnp.concatenate([zero_row, mixed_in[:-1]], axis=0), 0.0)
    back_two = jnp.where(
        position >= 2, jnp.concatenate([zero_row, zero_row, mixed_in[:-2]], axis=0), 0.0
    )
    taps = conv_taps.astype(jnp.float32)
    convolved = taps[0] * back_two + taps[1] * back_one + taps[2] * mixed_in
    return (outer_proj.astype(jnp.float32) * convolved).astype(jnp.bfloat16)


def shifted(values, axis, step):
    size = lax.axis_size(axis)
    return lax.ppermute(values, axis, [(i, (i + step) % size) for i in range(size)])


def spread(block, axis):
    size, me, rows = (lax.axis_size(axis), lax.axis_index(axis), block.shape[0])
    if size == 2:
        other = shifted(block, axis, 1)
        first = me == 0
        return jnp.concatenate([jnp.where(first, block, other), jnp.where(first, other, block)])
    whole = jnp.zeros((size * rows,) + block.shape[1:], block.dtype)
    for step in range(size):
        piece = block if step == 0 else shifted(block, axis, step)
        whole = lax.dynamic_update_slice_in_dim(whole, piece, (me - step) % size * rows, 0)
    return whole


def by_rep(block):
    return [block] + [shifted(block, "rep", step) for step in range(1, lax.axis_size("rep"))]


def group_rows(share_block):
    return jnp.concatenate([spread(block, "tp") for block in by_rep(share_block)])


def reduce_rows(partial, share):
    n_tp, tp, n_rep = (lax.axis_size("tp"), lax.axis_index("tp"), lax.axis_size("rep"))
    groups = partial.reshape(n_rep, n_tp, share, partial.shape[1])

    def chunk(step):
        return lax.dynamic_index_in_dim(groups, (tp + step) % n_tp, 1, keepdims=False)

    total = chunk(0).astype(jnp.float32)
    for step in range(1, n_tp):
        total = total + shifted(chunk(step), "tp", step).astype(jnp.float32)
    own = total[0]
    for step in range(1, n_rep):
        own = own + shifted(total[step].astype(jnp.bfloat16), "rep", -step).astype(jnp.float32)
    return own


def local(
    tokens,
    mix_gain,
    value_weight,
    outer_gate_weight,
    inner_gate_weight,
    conv_taps,
    mix_out_weight,
    ffn_gain,
    gate_weight,
    up_weight,
    down_weight,
):
    row_count = tokens.shape[0]
    share = row_count // lax.axis_size("tp")
    seq_len = row_count // SEQ_GRP
    n_rep, rep = (lax.axis_size("rep"), lax.axis_index("rep"))

    def part(array, axis):
        size = array.shape[axis] // n_rep
        return lax.dynamic_slice_in_dim(array, rep * size, size, axis)

    own_tokens = lax.dynamic_slice_in_dim(tokens, lax.axis_index("tp") * share, share, 0)
    conv_in = jnp.concatenate(
        [part(w, 1) for w in (value_weight, outer_gate_weight, inner_gate_weight)], axis=1
    )
    conv_full = lax.all_gather(conv_in, "fs", axis=0, tiled=True)
    mix_out_full = lax.all_gather(part(mix_out_weight, 0), "fs", axis=1, tiled=True)
    ffn_in = jnp.concatenate([part(w, 1) for w in (gate_weight, up_weight)], axis=1)
    ffn_full = lax.all_gather(ffn_in, "fs", axis=0, tiled=True)
    down_full = lax.all_gather(part(down_weight, 0), "fs", axis=1, tiled=True)
    normed = rms_norm(tokens, mix_gain)
    own_normed = lax.dynamic_slice_in_dim(normed, lax.axis_index("tp") * share, share, 0)
    rows = jnp.concatenate([normed] + [spread(b, "tp") for b in by_rep(own_normed)[1:]])
    proj = jnp.dot(rows, conv_full, preferred_element_type=jnp.float32).astype(jnp.bfloat16)
    value_proj, outer_proj, inner_proj = jnp.split(proj, 3, axis=1)
    mixed = short_conv(value_proj, outer_proj, inner_proj, part(conv_taps, 1), seq_len)
    mix_total = reduce_rows(
        jnp.dot(mixed, mix_out_full, preferred_element_type=jnp.float32).astype(jnp.bfloat16), share
    )
    after_mix = (own_tokens.astype(jnp.float32) + mix_total).astype(jnp.bfloat16)
    block_rows = group_rows(rms_norm(after_mix, ffn_gain))
    both = jnp.dot(block_rows, ffn_full, preferred_element_type=jnp.float32)
    gate_proj, up_proj = jnp.split(both, 2, axis=1)
    hidden = (jax.nn.silu(gate_proj) * up_proj).astype(jnp.bfloat16)
    ffn_total = reduce_rows(
        jnp.dot(hidden, down_full, preferred_element_type=jnp.float32).astype(jnp.bfloat16), share
    )
    finished = (after_mix.astype(jnp.float32) + ffn_total).astype(jnp.bfloat16)
    return spread(finished, "tp")


def solution(mesh):
    placed = (
        P(("rep", "fs"), None),
        P(),
        P("fs", "tp"),
        P("fs", "tp"),
        P("fs", "tp"),
        P(None, "tp"),
        P("tp", "fs"),
        P(),
        P("fs", "tp"),
        P("fs", "tp"),
        P("tp", "fs"),
    )
    return jax.shard_map(
        local, mesh=mesh, in_specs=placed, out_specs=P(("rep", "fs"), None), check_vma=False
    )
```

profile of v0, /device:TPU:0, one launch (start us, length us, event | category | flops | bytes accessed | tf_op | source)
XLA Modules:
  0.0 387.4 jit_solution(13555058826445362777)
XLA Ops:
  15.6 3.0 collective-permute-start
  18.6 23.3 %collective-permute-done = bf16[256,2048]{1,0:T(8,128)(2,1)} collective-permute-done((bf16[256,2048]{1,0:T(8,128)(2,1)S(1)}, bf16[256,2048]{1,0:T(8,128)(2,1)}, u32[]{:S(2)}, u32[]{:S(2)}) %collective-permute-start) | collective-permute-done | bytes 1048608 | tf_op jit(solution)/shard_map/ppermute | solution.py:32
  41.9 2.9 collective-permute-done.1
  44.9 3.0 broadcast_select_fusion.7
  47.9 43.9 %all-gather.5.cloned.1.call-done = bf16[2048,1152]{1,0:T(8,128)(2,1)} async-done(((bf16[256,1152]{1,0:T(8,128)(2,1)}), bf16[2048,1152]{1,0:T(8,128)(2,1)}) %all-gather.5.cloned.1.call-update) | async-done | bytes 4718608 | tf_op jit(solution)/shard_map/all_gather | solution.py:98
  91.8 9.8 %fusion.18 = bf16[1024,1152]{1,0:T(8,128)(2,1)S(1)} fusion(bf16[2048,1152]{1,0:T(8,128)(2,1)} %all-gather.5.cloned.1.call-done, bf16[256,2048]{1,0:T(8,128)(2,1)} %get-tuple-element.17, bf16[256,2048]{1,0:T(8,128)(2,1)} %get-tuple-element.16, bf16[512,2048]{1,0:T(8,128)(2,1)} %copy-done.3), kind=kOutput, calls=%fused_computation.24 | convolution fusion | flops 4845600768 | bytes 11272192 | tf_op jit(solution)/shard_map/dot_general | solution.py:106
  104.4 32.2 %all-gather.7.cloned.1.call-done = bf16[384,2048]{1,0:T(8,128)(2,1)} async-done(((bf16[384,256]{1,0:T(8,128)(2,1)}), bf16[384,2048]{1,0:T(8,128)(2,1)}) %all-gather.7.cloned.1.call-update) | async-done | bytes 1572880 | tf_op jit(solution)/shard_map/all_gather | solution.py:99
  136.6 6.0 %convolution_convert_fusion = bf16[1024,2048]{1,0:T(8,128)(2,1)S(1)} fusion(bf16[384,2048]{1,0:T(8,128)(2,1)} %all-gather.7.cloned.1.call-done, f32[1023,384]{1,0:T(8,128)} %bitcast.45, f32[1022,384]{1,0:T(8,128)} %bitcast.46, bf16[1024,1152]{1,0:T(8,128)(2,1)} %copy-done.5, f32[384]{0:T(512)S(1)} %get-tuple-element.6, f32[384]{0:T(512)S(1)} %get-tuple-element.7, ...), kind=kOutput, calls=%fused_computation.23 | convolution fusion | flops 1617821696 | bytes 11274240 | tf_op jit(solution)/shard_map/dot_general | solution.py:110
  142.7 2.0 copy-done.4
  144.7 1.6 dynamic-slice_bitcast_fusion.1
  147.1 3.6 collective-permute-done.2
  150.7 3.0 convert_add_fusion.1
  155.5 23.7 %collective-permute-done.3 = bf16[256,2048]{1,0:T(8,128)(2,1)S(1)} collective-permute-done((bf16[256,2048]{1,0:T(8,128)(2,1)S(1)}, bf16[256,2048]{1,0:T(8,128)(2,1)S(1)}, u32[]{:S(2)}, u32[]{:S(2)}) %collective-permute-start.3) | collective-permute-done | bytes 1048608 | tf_op jit(solution)/shard_map/ppermute | solution.py:32
  181.7 23.0 %collective-permute-done.5 = bf16[256,2048]{1,0:T(8,128)(2,1)S(1)} collective-permute-done((bf16[256,2048]{1,0:T(8,128)(2,1)S(1)}, bf16[256,2048]{1,0:T(8,128)(2,1)S(1)}, u32[]{:S(2)}, u32[]{:S(2)}) %collective-permute-start.5) | collective-permute-done | bytes 1048608 | tf_op jit(solution)/shard_map/ppermute | solution.py:32
  205.4 1.9 collective-permute-done.6
  208.8 52.6 %all-gather.9.cloned.1.call-done = bf16[2048,2048]{1,0:T(8,128)(2,1)} async-done(((bf16[256,2048]{1,0:T(8,128)(2,1)}), bf16[2048,2048]{1,0:T(8,128)(2,1)}) %all-gather.9.cloned.1.call-update) | async-done | bytes 8388624 | tf_op jit(solution)/shard_map/all_gather | solution.py:101
  261.5 13.8 %fusion.10 = f32[1024,2048]{1,0:T(8,128)} fusion(bf16[2048,2048]{1,0:T(8,128)(2,1)} %all-gather.9.cloned.1.call-done, bf16[256,2048]{1,0:T(8,128)(2,1)} %get-tuple-element.15, bf16[256,2048]{1,0:T(8,128)(2,1)} %get-tuple-element.14, bf16[256,2048]{1,0:T(8,128)(2,1)S(1)} %get-tuple-element.13, bf16[256,2048]{1,0:T(8,128)(2,1)S(1)} %get-tuple-element.12), kind=kOutput, calls=%fused_computation.13 | convolution fusion | flops 8606711808 | bytes 20971520 | tf_op jit(solution)/shard_map/dot_general | solution.py:114
  275.3 60.9 %all-gather.11.cloned.1.call-done = bf16[1024,2048]{1,0:T(8,128)(2,1)} async-done(((bf16[1024,256]{1,0:T(8,128)(2,1)}), bf16[1024,2048]{1,0:T(8,128)(2,1)}) %all-gather.11.cloned.1.call-update) | async-done | bytes 4194320 | tf_op jit(solution)/shard_map/all_gather | solution.py:102
  336.2 9.2 %convolution_convert_fusion.1 = bf16[1024,2048]{1,0:T(8,128)(2,1)S(1)} fusion(bf16[1024,2048]{1,0:T(8,128)(2,1)} %all-gather.11.cloned.1.call-done, f32[1024,2048]{1,0:T(8,128)} %fusion.10), kind=kOutput, calls=%fused_computation.25 | convolution fusion | flops 4303355904 | bytes 16777216 | tf_op jit(solution)/shard_map/dot_general | solution.py:118
  345.6 4.1 %collective-permute-done.7 = bf16[2,256,2048]{2,1,0:T(8,128)(2,1)S(1)} collective-permute-done((bf16[2,256,2048]{2,1,0:T(8,128)(2,1)S(1)}, bf16[2,256,2048]{2,1,0:T(8,128)(2,1)S(1)}, u32[]{:S(2)}, u32[]{:S(2)}) %collective-permute-start.7) | collective-permute-done | bytes 2097184 | tf_op jit(solution)/shard_map/ppermute | solution.py:32
  350.7 1.6 collective-permute-start.8
  352.3 23.7 %collective-permute-done.8 = bf16[256,2048]{1,0:T(8,128)(2,1)S(1)} collective-permute-done((bf16[256,2048]{1,0:T(8,128)(2,1)S(1)}, bf16[256,2048]{1,0:T(8,128)(2,1)S(1)}, u32[]{:S(2)}, u32[]{:S(2)}) %collective-permute-start.8) | collective-permute-done | bytes 1048608 | tf_op jit(solution)/shard_map/ppermute | solution.py:32
  376.5 2.6 collective-permute-done.9
  379.3 1.6 pad_maximum_fusion
  (64 shorter events, 20.7 us)
Async XLA Ops:
  6.5 139.7 %copy-start = (bf16[2048,256]{1,0:T(8,128)(2,1)S(1)}, bf16[2048,256]{1,0:T(8,128)(2,1)}, u32[]{:S(2)}) copy-start(bf16[2048,256]{1,0:T(8,128)(2,1)} %param.21) | copy-start | bytes 3145732
  6.5 3.1 copy-start.6
  6.5 85.3 %all-gather.5.cloned.1.call-start = ((), (), s32[]{:S(2)}) async-start(), calls=%async_computation | async-start | bytes 5308416 | tf_op jit(solution)/shard_map/all_gather | solution.py:98
  9.6 127.1 %all-gather.7.cloned.1.call-start = ((), (), s32[]{:S(2)}) async-start(), calls=%async_computation.1 | async-start | bytes 1769472 | tf_op jit(solution)/shard_map/all_gather | solution.py:99
  10.4 251.1 %all-gather.9.cloned.1.call-start = ((), (), s32[]{:S(2)}) async-start(), calls=%async_computation.2 | async-start | bytes 9437184 | tf_op jit(solution)/shard_map/all_gather | solution.py:101
  10.4 2.6 copy-start.7
  10.4 2.6 copy-start.2
  13.0 323.2 %all-gather.11.cloned.1.call-start = ((), (), s32[]{:S(2)}) async-start(), calls=%async_computation.3 | async-start | bytes 4718592 | tf_op jit(solution)/shard_map/all_gather | solution.py:102
  13.6 28.3 %copy-start.9 = (bf16[3,768]{1,0:T(4,128)(2,1)S(1)}, bf16[3,768]{1,0:T(4,128)(2,1)}, u32[]{:S(2)}) copy-start(bf16[3,768]{1,0:T(4,128)(2,1)} %param.16) | copy-start | bytes 13828
  14.1 1.3 copy-start.3
  15.6 26.3 %collective-permute-start = (bf16[256,2048]{1,0:T(8,128)(2,1)S(1)}, bf16[256,2048]{1,0:T(8,128)(2,1)}, u32[]{:S(2)}, u32[]{:S(2)}) collective-permute-start(bf16[256,2048]{1,0:T(8,128)(2,1)S(1)} %constant_dynamic-slice_fusion.8), channel_id=1, source_target_pairs={{0,16},{16,0},{1,17},{17,1},{2,18},{18,2},{3,19},{19,3},{4,20},{20... | collective-permute-start | bytes 3145736 | tf_op jit(solution)/shard_map/ppermute | solution.py:32
  41.9 3.0 collective-permute-start.1
  101.6 1.5 copy-start.5
  142.7 2.0 copy-start.4
  146.2 4.5 %collective-permute-start.2 = (bf16[2,256,2048]{2,1,0:T(8,128)(2,1)}, bf16[2,256,2048]{2,1,0:T(8,128)(2,1)}, u32[]{:S(2)}, u32[]{:S(2)}) collective-permute-start(bf16[2,256,2048]{2,1,0:T(8,128)(2,1)} %dynamic-slice_bitcast_fusion.1), channel_id=1, source_target_pairs={{0,1},{1,0},{2,3},{3,2},{4,5},{5,4},{6,7},{7,6},{8,9},{9,8},{10,11... | collective-permute-start | bytes 6291464 | tf_op jit(solution)/shard_map/ppermute | solution.py:32
  147.1 8.4 %copy-start.8 = (bf16[2048]{0:T(1024)(128)(2,1)S(1)}, bf16[2048]{0:T(1024)(128)(2,1)}, u32[]{:S(2)}) copy-start(bf16[2048]{0:T(1024)(128)(2,1)} %param.18) | copy-start | bytes 12292
  153.9 25.3 %collective-permute-start.3 = (bf16[256,2048]{1,0:T(8,128)(2,1)S(1)}, bf16[256,2048]{1,0:T(8,128)(2,1)S(1)}, u32[]{:S(2)}, u32[]{:S(2)}) collective-permute-start(bf16[256,2048]{1,0:T(8,128)(2,1)S(1)} %fusion.31), channel_id=1, source_target_pairs={{0,16},{16,0},{1,17},{17,1},{2,18},{18,2},{3,19},{19,3},{4,20},{20... | collective-permute-start | bytes 3145736 | tf_op jit(solution)/shard_map/ppermute | solution.py:32
  180.2 24.5 %collective-permute-start.5 = (bf16[256,2048]{1,0:T(8,128)(2,1)S(1)}, bf16[256,2048]{1,0:T(8,128)(2,1)S(1)}, u32[]{:S(2)}, u32[]{:S(2)}) collective-permute-start(bf16[256,2048]{1,0:T(8,128)(2,1)S(1)} %fusion.23), channel_id=1, source_target_pairs={{0,16},{16,0},{1,17},{17,1},{2,18},{18,2},{3,19},{19,3},{4,20},{20... | collective-permute-start | bytes 3145736 | tf_op jit(solution)/shard_map/ppermute | solution.py:32
  181.7 23.0 %collective-permute-start.4 = (bf16[256,2048]{1,0:T(8,128)(2,1)S(1)}, bf16[256,2048]{1,0:T(8,128)(2,1)S(1)}, u32[]{:S(2)}, u32[]{:S(2)}) collective-permute-start(bf16[256,2048]{1,0:T(8,128)(2,1)S(1)} %fusion.23), channel_id=1, source_target_pairs={{0,1},{1,0},{2,3},{3,2},{4,5},{5,4},{6,7},{7,6},{8,9},{9,8},{10,11... | collective-permute-start | bytes 3145736 | tf_op jit(solution)/shard_map/ppermute | solution.py:32
  204.7 2.7 collective-permute-start.6
  345.6 4.2 %collective-permute-start.7 = (bf16[2,256,2048]{2,1,0:T(8,128)(2,1)S(1)}, bf16[2,256,2048]{2,1,0:T(8,128)(2,1)S(1)}, u32[]{:S(2)}, u32[]{:S(2)}) collective-permute-start(bf16[2,256,2048]{2,1,0:T(8,128)(2,1)S(1)} %dynamic-slice_bitcast_fusion), channel_id=1, source_target_pairs={{0,1},{1,0},{2,3},{3,2},{4,5},{5,4},{6,7},{7,6},{8,9},{9,8},{10,11... | collective-permute-start | bytes 6291464 | tf_op jit(solution)/shard_map/ppermute | solution.py:32
  350.7 25.3 %collective-permute-start.8 = (bf16[256,2048]{1,0:T(8,128)(2,1)S(1)}, bf16[256,2048]{1,0:T(8,128)(2,1)S(1)}, u32[]{:S(2)}, u32[]{:S(2)}) collective-permute-start(bf16[256,2048]{1,0:T(8,128)(2,1)S(1)} %fusion.32), channel_id=1, source_target_pairs={{0,16},{16,0},{1,17},{17,1},{2,18},{18,2},{3,19},{19,3},{4,20},{20... | collective-permute-start | bytes 3145736 | tf_op jit(solution)/shard_map/ppermute | solution.py:32
  376.5 2.7 collective-permute-start.9
  379.2 1.7 copy-start.1
Sparse Core Ops, SparseCore 0:
  9.7 82.0 all-gather.4
  93.8 42.7 all-gather.6
  138.8 122.6 all-gather.8
  263.4 72.8 all-gather.10
where the time goes:
time: 388 us; the launch traced here: 387 us
  waiting for transfers between devices  299 us (77%)
  matrix products  38.9 us (10%)
  other arithmetic  16.5 us (4%)
  between operations  13.4 us (3%)
  local copies, waits for them, and re-layouts  12 us (3%)
  starting transfers between devices  7.97 us (2%)
    ppermute x10, waiting for transfers between devices, shifted(): lax.ppermute(values, axis, [(i, (i + step) % size) for i in range(size)])  109 us
    all_gather x1, waiting for transfers between devices, local(): down_full = lax.all_gather(part(down_weight, 0), 'fs', axis=1, tiled=True)  60.9 us
    all_gather x1, waiting for transfers between devices, local(): ffn_full = lax.all_gather(ffn_in, 'fs', axis=0, tiled=True)  52.6 us
    all_gather x1, waiting for transfers between devices, local(): conv_full = lax.all_gather(conv_in, 'fs', axis=0, tiled=True)  43.9 us
    all_gather x1, waiting for transfers between devices, local(): lax.all_gather(part(mix_out_weight, 0), 'fs', axis=1, tiled=True)  32.2 us
    dot_general x1, matrix products, local(): both = jnp.dot(block_rows, ffn_full, preferred_element_type=jnp.float32)  13.8 us
    dot_general x1, matrix products, local(): jnp.dot(rows, conv_full, preferred_element_type=jnp.float32)  9.83 us
    dot_general x1, matrix products, local(): jnp.dot(hidden, down_full, preferred_element_type=jnp.float32)  9.19 us
  transfers between devices with their start and end apart: 14, of which 13 were waited for; matrix products, arithmetic and copies ran while one was open for 12% of the time, Pallas kernels for 0%

commit v1 on v0

--- a/solution.py
+++ b/solution.py
@@ -95,7 +95,18 @@
     conv_in = jnp.concatenate(
         [part(w, 1) for w in (value_weight, outer_gate_weight, inner_gate_weight)], axis=1
     )
-    conv_full = lax.all_gather(conv_in, "fs", axis=0, tiled=True)
+    extent = jax.lax.axis_size("fs")
+    top = conv_in
+    w1 = [(dd - 1, dd) for dd in range(1, extent)] + [(extent - 1, 0)]
+    crops = [top]
+    for _ in range(extent - 1):
+        top = jax.lax.ppermute(top, "fs", w1)
+        crops += [top]
+    conv_full = jnp.roll(
+        jnp.concatenate([*reversed(crops)], axis=0),
+        (jax.lax.axis_index("fs") + 1) * top.shape[0],
+        axis=0,
+    )
     mix_out_full = lax.all_gather(part(mix_out_weight, 0), "fs", axis=1, tiled=True)
     ffn_in = jnp.concatenate([part(w, 1) for w in (gate_weight, up_weight)], axis=1)
     ffn_full = lax.all_gather(ffn_in, "fs", axis=0, tiled=True)

time: 388 us -> 363 us (0.936)
  waiting for transfers between devices: 299 us -> 269 us
  local copies, waits for them, and re-layouts: 12 us -> 20.3 us
    ppermute x0 -> x7, waiting for transfers between devices: none -> 160 us  [local(): top = jax.lax.ppermute(top, 'fs', w1)]
    all_gather x1, waiting for transfers between devices: 52.6 us -> 0.01 us  [local(): ffn_full = lax.all_gather(ffn_in, 'fs', axis=0, tiled=True)]
    all_gather x1 -> x0, waiting for transfers between devices: 43.9 us -> none  [local(): conv_full = lax.all_gather(conv_in, 'fs', axis=0, tiled=True)]
    all_gather x1, waiting for transfers between devices: 60.9 us -> 25 us  [local(): down_full = lax.all_gather(part(down_weight, 0), 'fs', axis=1, tiled=True)]
    all_gather x1, waiting for transfers between devices: 32.2 us -> 0.02 us  [local(): lax.all_gather(part(mix_out_weight, 0), 'fs', axis=1, tiled=True)]
    ppermute x10, waiting for transfers between devices: 109 us -> 83.9 us  [shifted(): lax.ppermute(values, axis, [(i, (i + step) % size) for i in range(size)])]
    unnamed x20 -> x42, local copies, waits for them, and re-layouts: 4.81 us -> 12.5 us
  transfers between devices with their start and end apart: 14 -> 20, of which waited for: 13 -> 15; matrix products, arithmetic and copies ran while one was open for 12% -> 14% of each run, Pallas kernels for 0% -> 0%
where the time goes in v1:
time: 363 us; the launch traced here: 362 us
  waiting for transfers between devices  269 us (74%)
  matrix products  36.6 us (10%)
  local copies, waits for them, and re-layouts  20.3 us (6%)
  other arithmetic  14.7 us (4%)
  between operations  13.6 us (4%)
  starting transfers between devices  7.89 us (2%)
    ppermute x7, waiting for transfers between devices, local(): top = jax.lax.ppermute(top, 'fs', w1)  160 us
    ppermute x10, waiting for transfers between devices, shifted(): lax.ppermute(values, axis, [(i, (i + step) % size) for i in range(size)])  83.9 us
    all_gather x1, waiting for transfers between devices, local(): down_full = lax.all_gather(part(down_weight, 0), 'fs', axis=1, tiled=True)  25 us
    dot_general x1, matrix products, local(): both = jnp.dot(block_rows, ffn_full, preferred_element_type=jnp.float32)  14.1 us
    unnamed x42, local copies, waits for them, and re-layouts  12.5 us
    dot_general x1, matrix products, local(): jnp.dot(hidden, down_full, preferred_element_type=jnp.float32)  9.19 us
    dot_general x1, matrix products, local(): jnp.dot(rows, conv_full, preferred_element_type=jnp.float32)  8.16 us
  transfers between devices with their start and end apart: 20, of which 15 were waited for; matrix products, arithmetic and copies ran while one was open for 14% of the time, Pallas kernels for 0%

profile of v1, /device:TPU:0, one launch (start us, length us, event | category | flops | bytes accessed | tf_op | source)
XLA Modules:
  0.0 362.1 jit_solution(5485506010560912385)
XLA Ops:
  6.6 1.8 constant_dynamic-slice_fusion.3
  13.6 3.0 collective-permute-start.2
  16.7 22.3 %collective-permute-done.2 = bf16[256,1152]{1,0:T(8,128)(2,1)S(1)} collective-permute-done((bf16[256,1152]{1,0:T(8,128)(2,1)S(1)}, bf16[256,1152]{1,0:T(8,128)(2,1)S(1)}, u32[]{:S(2)}, u32[]{:S(2)}) %collective-permute-start.2) | collective-permute-done | bytes 589856 | tf_op jit(solution)/shard_map/ppermute | solution.py:103
  40.4 25.9 %collective-permute-done.3 = bf16[256,1152]{1,0:T(8,128)(2,1)} collective-permute-done((bf16[256,1152]{1,0:T(8,128)(2,1)S(1)}, bf16[256,1152]{1,0:T(8,128)(2,1)}, u32[]{:S(2)}, u32[]{:S(2)}) %collective-permute-start.3) | collective-permute-done | bytes 589856 | tf_op jit(solution)/shard_map/ppermute | solution.py:103
  66.3 1.9 fusion.4
  70.9 10.1 %collective-permute-done.4 = bf16[256,1152]{1,0:T(8,128)(2,1)} collective-permute-done((bf16[256,1152]{1,0:T(8,128)(2,1)}, bf16[256,1152]{1,0:T(8,128)(2,1)}, u32[]{:S(2)}, u32[]{:S(2)}) %collective-permute-start.4) | collective-permute-done | bytes 589856 | tf_op jit(solution)/shard_map/ppermute | solution.py:103
  81.0 29.9 %collective-permute-done.5 = bf16[256,1152]{1,0:T(8,128)(2,1)S(1)} collective-permute-done((bf16[256,1152]{1,0:T(8,128)(2,1)}, bf16[256,1152]{1,0:T(8,128)(2,1)S(1)}, u32[]{:S(2)}, u32[]{:S(2)}) %collective-permute-start.5) | collective-permute-done | bytes 589856 | tf_op jit(solution)/shard_map/ppermute | solution.py:103
  111.0 29.7 %collective-permute-done.6 = bf16[256,1152]{1,0:T(8,128)(2,1)S(1)} collective-permute-done((bf16[256,1152]{1,0:T(8,128)(2,1)S(1)}, bf16[256,1152]{1,0:T(8,128)(2,1)S(1)}, u32[]{:S(2)}, u32[]{:S(2)}) %collective-permute-start.6) | collective-permute-done | bytes 589856 | tf_op jit(solution)/shard_map/ppermute | solution.py:103
  140.7 14.9 %collective-permute-done.7 = bf16[256,1152]{1,0:T(8,128)(2,1)S(1)} collective-permute-done((bf16[256,1152]{1,0:T(8,128)(2,1)S(1)}, bf16[256,1152]{1,0:T(8,128)(2,1)S(1)}, u32[]{:S(2)}, u32[]{:S(2)}) %collective-permute-start.7) | collective-permute-done | bytes 589856 | tf_op jit(solution)/shard_map/ppermute | solution.py:103
  157.4 27.2 %collective-permute-done.8 = bf16[256,1152]{1,0:T(8,128)(2,1)} collective-permute-done((bf16[256,1152]{1,0:T(8,128)(2,1)S(1)}, bf16[256,1152]{1,0:T(8,128)(2,1)}, u32[]{:S(2)}, u32[]{:S(2)}) %collective-permute-start.8) | collective-permute-done | bytes 589856 | tf_op jit(solution)/shard_map/ppermute | solution.py:103
  192.4 8.2 %fusion.19 = bf16[1024,1152]{1,0:T(8,128)(2,1)S(1)} fusion(bf16[4096,1152]{1,0:T(8,128)(2,1)S(1)} %constant_dynamic-update-slice_fusion, s32[]{:T(128)S(6)} %select_n.116, bf16[256,2048]{1,0:T(8,128)(2,1)S(1)} %get-tuple-element.17, bf16[256,2048]{1,0:T(8,128)(2,1)S(1)} %get-tuple-element.16, bf16[512,2048]{1,0:T(8,128)(2,1)S(1)} %copy-done.4), kind=kOutput, calls=%fused_computation.25 | convolution fusion | flops 4845600768 | bytes 11272196 | tf_op jit(solution)/shard_map/dot_general | solution.py:117
  202.2 5.1 %convolution_convert_fusion = bf16[1024,2048]{1,0:T(8,128)(2,1)S(1)} fusion(bf16[384,2048]{1,0:T(8,128)(2,1)} %all-gather.4.cloned.1.call-done, f32[1023,384]{1,0:T(8,128)S(1)} %bitcast.44, f32[1022,384]{1,0:T(8,128)S(1)} %bitcast.45, bf16[1024,1152]{1,0:T(8,128)(2,1)} %copy-done.10, f32[384]{0:T(512)S(1)} %get-tuple-element.6, ...), kind=kOutput, calls=%fused_computation.24 | convolution fusion | flops 1617821696 | bytes 11274240 | tf_op jit(solution)/shard_map/dot_general | solution.py:121
  207.3 2.0 copy-done.5
  210.5 3.4 collective-permute-done.9
  213.8 3.0 convert_add_fusion.1
  217.8 24.5 %collective-permute-done.10 = bf16[256,2048]{1,0:T(8,128)(2,1)S(1)} collective-permute-done((bf16[256,2048]{1,0:T(8,128)(2,1)S(1)}, bf16[256,2048]{1,0:T(8,128)(2,1)S(1)}, u32[]{:S(2)}, u32[]{:S(2)}) %collective-permute-start.10) | collective-permute-done | bytes 1048608 | tf_op jit(solution)/shard_map/ppermute | solution.py:32
  244.0 23.7 %collective-permute-done.12 = bf16[256,2048]{1,0:T(8,128)(2,1)S(1)} collective-permute-done((bf16[256,2048]{1,0:T(8,128)(2,1)S(1)}, bf16[256,2048]{1,0:T(8,128)(2,1)S(1)}, u32[]{:S(2)}, u32[]{:S(2)}) %collective-permute-start.12) | collective-permute-done | bytes 1048608 | tf_op jit(solution)/shard_map/ppermute | solution.py:32
  268.3 1.9 collective-permute-done.13
  271.8 14.1 %fusion.11 = f32[1024,2048]{1,0:T(8,128)} fusion(bf16[2048,2048]{1,0:T(8,128)(2,1)} %all-gather.6.cloned.1.call-done, bf16[256,2048]{1,0:T(8,128)(2,1)} %get-tuple-element.15, bf16[256,2048]{1,0:T(8,128)(2,1)} %get-tuple-element.14, bf16[256,2048]{1,0:T(8,128)(2,1)S(1)} %get-tuple-element.13, bf16[256,2048]{1,0:T(8,128)(2,1)S(1)} %get-tuple-element.12), kind=kOutput, calls=%fused_computation.14 | convolution fusion | flops 8606711808 | bytes 20971520 | tf_op jit(solution)/shard_map/dot_general | solution.py:125
  285.9 25.0 %all-gather.8.cloned.1.call-done = bf16[1024,2048]{1,0:T(8,128)(2,1)} async-done(((bf16[1024,256]{1,0:T(8,128)(2,1)}), bf16[1024,2048]{1,0:T(8,128)(2,1)}) %all-gather.8.cloned.1.call-update) | async-done | bytes 4194320 | tf_op jit(solution)/shard_map/all_gather | solution.py:113
  310.9 9.2 %convolution_convert_fusion.1 = bf16[1024,2048]{1,0:T(8,128)(2,1)S(1)} fusion(bf16[1024,2048]{1,0:T(8,128)(2,1)} %all-gather.8.cloned.1.call-done, f32[1024,2048]{1,0:T(8,128)} %fusion.11), kind=kOutput, calls=%fused_computation.26 | convolution fusion | flops 4303355904 | bytes 16777216 | tf_op jit(solution)/shard_map/dot_general | solution.py:129
  320.3 4.1 %collective-permute-done.14 = bf16[2,256,2048]{2,1,0:T(8,128)(2,1)S(1)} collective-permute-done((bf16[2,256,2048]{2,1,0:T(8,128)(2,1)S(1)}, bf16[2,256,2048]{2,1,0:T(8,128)(2,1)S(1)}, u32[]{:S(2)}, u32[]{:S(2)}) %collective-permute-start.14) | collective-permute-done | bytes 2097184 | tf_op jit(solution)/shard_map/ppermute | solution.py:32
  327.0 23.7 %collective-permute-done.15 = bf16[256,2048]{1,0:T(8,128)(2,1)S(1)} collective-permute-done((bf16[256,2048]{1,0:T(8,128)(2,1)S(1)}, bf16[256,2048]{1,0:T(8,128)(2,1)S(1)}, u32[]{:S(2)}, u32[]{:S(2)}) %collective-permute-start.15) | collective-permute-done | bytes 1048608 | tf_op jit(solution)/shard_map/ppermute | solution.py:32
  351.2 2.6 collective-permute-done.16
  (99 shorter events, 31.2 us)
Async XLA Ops:
  6.5 203.0 %copy-start = (bf16[2048,256]{1,0:T(8,128)(2,1)S(1)}, bf16[2048,256]{1,0:T(8,128)(2,1)}, u32[]{:S(2)}) copy-start(bf16[2048,256]{1,0:T(8,128)(2,1)} %param.21) | copy-start | bytes 3145732
  6.5 33.3 %copy-start.11 = (bf16[2048]{0:T(1024)(128)(2,1)S(1)}, bf16[2048]{0:T(1024)(128)(2,1)}, u32[]{:S(2)}) copy-start(bf16[2048]{0:T(1024)(128)(2,1)} %param.12) | copy-start | bytes 12292
  6.5 33.3 %copy-start.2 = (bf16[512,2048]{1,0:T(8,128)(2,1)S(1)}, bf16[512,2048]{1,0:T(8,128)(2,1)}, u32[]{:S(2)}) copy-start(bf16[512,2048]{1,0:T(8,128)(2,1)} %param.11) | copy-start | bytes 6291460
  6.5 195.6 %all-gather.4.cloned.1.call-start = ((), (), s32[]{:S(2)}) async-start(), calls=%async_computation | async-start | bytes 1769472 | tf_op jit(solution)/shard_map/all_gather | solution.py:110
  8.4 263.5 %all-gather.6.cloned.1.call-start = ((), (), s32[]{:S(2)}) async-start(), calls=%async_computation.1 | async-start | bytes 9437184 | tf_op jit(solution)/shard_map/all_gather | solution.py:112
  10.8 300.1 %all-gather.8.cloned.1.call-start = ((), (), s32[]{:S(2)}) async-start(), calls=%async_computation.2 | async-start | bytes 4718592 | tf_op jit(solution)/shard_map/all_gather | solution.py:113
  13.6 25.4 %collective-permute-start.2 = (bf16[256,1152]{1,0:T(8,128)(2,1)S(1)}, bf16[256,1152]{1,0:T(8,128)(2,1)S(1)}, u32[]{:S(2)}, u32[]{:S(2)}) collective-permute-start(bf16[256,1152]{1,0:T(8,128)(2,1)S(1)} %pad_maximum_fusion.2), channel_id=1, source_target_pairs={{0,2},{2,4},{4,6},{6,8},{8,10},{10,12},{12,14},{14,0},{1,3},{3,5},... | collective-permute-start | bytes 1769480 | tf_op jit(solution)/shard_map/ppermute | solution.py:103
  39.8 26.5 %collective-permute-start.3 = (bf16[256,1152]{1,0:T(8,128)(2,1)S(1)}, bf16[256,1152]{1,0:T(8,128)(2,1)}, u32[]{:S(2)}, u32[]{:S(2)}) collective-permute-start(bf16[256,1152]{1,0:T(8,128)(2,1)S(1)} %collective-permute-done.2), channel_id=1, source_target_pairs={{0,2},{2,4},{4,6},{6,8},{8,10},{10,12},{12,14},{14,0},{1,3},{3,5},... | collective-permute-start | bytes 1769480 | tf_op jit(solution)/shard_map/ppermute | solution.py:103
  39.9 100.9 %copy-start.13 = (bf16[3,768]{1,0:T(4,128)(2,1)S(1)}, bf16[3,768]{1,0:T(4,128)(2,1)}, u32[]{:S(2)}) copy-start(bf16[3,768]{1,0:T(4,128)(2,1)} %param.16) | copy-start | bytes 13828
  66.3 14.7 %collective-permute-start.4 = (bf16[256,1152]{1,0:T(8,128)(2,1)}, bf16[256,1152]{1,0:T(8,128)(2,1)}, u32[]{:S(2)}, u32[]{:S(2)}) collective-permute-start(bf16[256,1152]{1,0:T(8,128)(2,1)} %collective-permute-done.3), channel_id=1, source_target_pairs={{0,2},{2,4},{4,6},{6,8},{8,10},{10,12},{12,14},{14,0},{1,3},{3,5},... | collective-permute-start | bytes 1769480 | tf_op jit(solution)/shard_map/ppermute | solution.py:103
  69.5 41.5 %collective-permute-start = (bf16[256,2048]{1,0:T(8,128)(2,1)S(1)}, bf16[256,2048]{1,0:T(8,128)(2,1)}, u32[]{:S(2)}, u32[]{:S(2)}) collective-permute-start(bf16[256,2048]{1,0:T(8,128)(2,1)S(1)} %constant_dynamic-slice_fusion.8), channel_id=1, source_target_pairs={{0,16},{16,0},{1,17},{17,1},{2,18},{18,2},{3,19},{19,3},{4,20},{20... | collective-permute-start | bytes 3145736 | tf_op jit(solution)/shard_map/ppermute | solution.py:32
  81.0 29.9 %collective-permute-start.5 = (bf16[256,1152]{1,0:T(8,128)(2,1)}, bf16[256,1152]{1,0:T(8,128)(2,1)S(1)}, u32[]{:S(2)}, u32[]{:S(2)}) collective-permute-start(bf16[256,1152]{1,0:T(8,128)(2,1)} %collective-permute-done.4), channel_id=1, source_target_pairs={{0,2},{2,4},{4,6},{6,8},{8,10},{10,12},{12,14},{14,0},{1,3},{3,5},... | collective-permute-start | bytes 1769480 | tf_op jit(solution)/shard_map/ppermute | solution.py:103
  111.0 29.7 %collective-permute-start.6 = (bf16[256,1152]{1,0:T(8,128)(2,1)S(1)}, bf16[256,1152]{1,0:T(8,128)(2,1)S(1)}, u32[]{:S(2)}, u32[]{:S(2)}) collective-permute-start(bf16[256,1152]{1,0:T(8,128)(2,1)S(1)} %collective-permute-done.5), channel_id=1, source_target_pairs={{0,2},{2,4},{4,6},{6,8},{8,10},{10,12},{12,14},{14,0},{1,3},{3,5},... | collective-permute-start | bytes 1769480 | tf_op jit(solution)/shard_map/ppermute | solution.py:103
  111.0 44.7 %collective-permute-start.1 = (bf16[256,2048]{1,0:T(8,128)(2,1)}, bf16[256,2048]{1,0:T(8,128)(2,1)}, u32[]{:S(2)}, u32[]{:S(2)}) collective-permute-start(bf16[256,2048]{1,0:T(8,128)(2,1)} %collective-permute-done), channel_id=1, source_target_pairs={{0,1},{1,0},{2,3},{3,2},{4,5},{5,4},{6,7},{7,6},{8,9},{9,8},{10,11... | collective-permute-start | bytes 3145736 | tf_op jit(solution)/shard_map/ppermute | solution.py:32
  140.7 14.9 %collective-permute-start.7 = (bf16[256,1152]{1,0:T(8,128)(2,1)S(1)}, bf16[256,1152]{1,0:T(8,128)(2,1)S(1)}, u32[]{:S(2)}, u32[]{:S(2)}) collective-permute-start(bf16[256,1152]{1,0:T(8,128)(2,1)S(1)} %collective-permute-done.6), channel_id=1, source_target_pairs={{0,2},{2,4},{4,6},{6,8},{8,10},{10,12},{12,14},{14,0},{1,3},{3,5},... | collective-permute-start | bytes 1769480 | tf_op jit(solution)/shard_map/ppermute | solution.py:103
  155.6 29.0 %collective-permute-start.8 = (bf16[256,1152]{1,0:T(8,128)(2,1)S(1)}, bf16[256,1152]{1,0:T(8,128)(2,1)}, u32[]{:S(2)}, u32[]{:S(2)}) collective-permute-start(bf16[256,1152]{1,0:T(8,128)(2,1)S(1)} %collective-permute-done.7), channel_id=1, source_target_pairs={{0,2},{2,4},{4,6},{6,8},{8,10},{10,12},{12,14},{14,0},{1,3},{3,5},... | collective-permute-start | bytes 1769480 | tf_op jit(solution)/shard_map/ppermute | solution.py:103
  209.5 4.4 %collective-permute-start.9 = (bf16[2,256,2048]{2,1,0:T(8,128)(2,1)S(1)}, bf16[2,256,2048]{2,1,0:T(8,128)(2,1)}, u32[]{:S(2)}, u32[]{:S(2)}) collective-permute-start(bf16[2,256,2048]{2,1,0:T(8,128)(2,1)S(1)} %dynamic-slice_bitcast_fusion.1), channel_id=1, source_target_pairs={{0,1},{1,0},{2,3},{3,2},{4,5},{5,4},{6,7},{7,6},{8,9},{9,8},{10,11... | collective-permute-start | bytes 6291464 | tf_op jit(solution)/shard_map/ppermute | solution.py:32
  217.0 25.3 %collective-permute-start.10 = (bf16[256,2048]{1,0:T(8,128)(2,1)S(1)}, bf16[256,2048]{1,0:T(8,128)(2,1)S(1)}, u32[]{:S(2)}, u32[]{:S(2)}) collective-permute-start(bf16[256,2048]{1,0:T(8,128)(2,1)S(1)} %fusion.34), channel_id=1, source_target_pairs={{0,16},{16,0},{1,17},{17,1},{2,18},{18,2},{3,19},{19,3},{4,20},{20... | collective-permute-start | bytes 3145736 | tf_op jit(solution)/shard_map/ppermute | solution.py:32
  243.2 24.4 %collective-permute-start.12 = (bf16[256,2048]{1,0:T(8,128)(2,1)S(1)}, bf16[256,2048]{1,0:T(8,128)(2,1)S(1)}, u32[]{:S(2)}, u32[]{:S(2)}) collective-permute-start(bf16[256,2048]{1,0:T(8,128)(2,1)S(1)} %fusion.26), channel_id=1, source_target_pairs={{0,16},{16,0},{1,17},{17,1},{2,18},{18,2},{3,19},{19,3},{4,20},{20... | collective-permute-start | bytes 3145736 | tf_op jit(solution)/shard_map/ppermute | solution.py:32
  243.9 23.7 %collective-permute-start.11 = (bf16[256,2048]{1,0:T(8,128)(2,1)S(1)}, bf16[256,2048]{1,0:T(8,128)(2,1)S(1)}, u32[]{:S(2)}, u32[]{:S(2)}) collective-permute-start(bf16[256,2048]{1,0:T(8,128)(2,1)S(1)} %fusion.26), channel_id=1, source_target_pairs={{0,1},{1,0},{2,3},{3,2},{4,5},{5,4},{6,7},{7,6},{8,9},{9,8},{10,11... | collective-permute-start | bytes 3145736 | tf_op jit(solution)/shard_map/ppermute | solution.py:32
  267.6 2.7 collective-permute-start.13
  320.2 4.2 %collective-permute-start.14 = (bf16[2,256,2048]{2,1,0:T(8,128)(2,1)S(1)}, bf16[2,256,2048]{2,1,0:T(8,128)(2,1)S(1)}, u32[]{:S(2)}, u32[]{:S(2)}) collective-permute-start(bf16[2,256,2048]{2,1,0:T(8,128)(2,1)S(1)} %dynamic-slice_bitcast_fusion), channel_id=1, source_target_pairs={{0,1},{1,0},{2,3},{3,2},{4,5},{5,4},{6,7},{7,6},{8,9},{9,8},{10,11... | collective-permute-start | bytes 6291464 | tf_op jit(solution)/shard_map/ppermute | solution.py:32
  325.4 25.3 %collective-permute-start.15 = (bf16[256,2048]{1,0:T(8,128)(2,1)S(1)}, bf16[256,2048]{1,0:T(8,128)(2,1)S(1)}, u32[]{:S(2)}, u32[]{:S(2)}) collective-permute-start(bf16[256,2048]{1,0:T(8,128)(2,1)S(1)} %fusion.35), channel_id=1, source_target_pairs={{0,16},{16,0},{1,17},{17,1},{2,18},{18,2},{3,19},{19,3},{4,20},{20... | collective-permute-start | bytes 3145736 | tf_op jit(solution)/shard_map/ppermute | solution.py:32
  351.1 2.7 collective-permute-start.16
  (10 other events, 113.7 us)
Sparse Core Ops, SparseCore 0:
  9.4 59.2 all-gather.3
  70.8 164.1 all-gather.5
  237.1 73.7 all-gather.7
